TPU v7x, 32 devices: a whole 2x2x4 slice. The times are simulated.
32 devices in a mesh: dp: 4 (over y, x), kv: 4 (over z), tp: 2 (over core).
Axes of the slice: x: 2, y: 2, z: 4, core: 2. Of those that a mesh axis runs over, the one named last changes fastest.
Arguments:
- tokens: bfloat16 [128, 2048], P('dp', 'kv'), may hold values from -18 to 18
- mix_gain: float32 [2048], P('kv'), may hold values from 0.1 to 1.9
- w_query: bfloat16 [2048, 1024], P('kv', 'tp'), may hold values from -0.125 to 0.125
- w_key: bfloat16 [2048, 1024], P('kv', 'tp'), may hold values from -0.125 to 0.125
- w_value: bfloat16 [2048, 2048], P('kv', 'tp'), may hold values from -0.125 to 0.125
- w_outgate: bfloat16 [2048, 2048], P('kv', 'tp'), may hold values from -0.125 to 0.125
- w_gates: bfloat16 [2048, 16], replicated, may hold values from -0.25 to 0.25
- forget_bias: float32 [8], P('tp'), may hold values from -1 to 3
- memory: float32 [128, 8, 128, 256], P(('dp', 'kv'), 'tp'), may hold values from -4 to 4
- normalizer: float32 [128, 8, 128], P(('dp', 'kv'), 'tp'), may hold values from -4 to 4
- stabilizer: float32 [128, 8], P(('dp', 'kv'), 'tp'), may hold values from -4 to 4
- head_gain: float32 [8, 256], P('tp'), may hold values from 0.1 to 1.9
- w_out: bfloat16 [2048, 2048], P('tp', 'kv'), may hold values from -0.125 to 0.125
- mlp_gain: float32 [2048], replicated, may hold values from 0.1 to 1.9
- w_gate: bfloat16 [2048, 5632], P(None, ('kv', 'tp')), may hold values from -0.125 to 0.125
- w_up: bfloat16 [2048, 5632], P(None, ('kv', 'tp')), may hold values from -0.125 to 0.125
- w_down: bfloat16 [5632, 2048], P(('kv', 'tp')), may hold values from -0.109375 to 0.109375
Outputs:
- mixed_out: bfloat16 [128, 2048], P('dp', ('kv', 'tp'))
- new_memory: float32 [128, 8, 128, 256], P(('dp', 'kv'), 'tp')
- new_normalizer: float32 [128, 8, 128], P(('dp', 'kv'), 'tp')
- new_stabilizer: float32 [128, 8], P(('dp', 'kv'), 'tp')
All inputs are finite; a program needn't handle non-finite values.
Results may differ from a plain program's by a relative error of at most 0.02.
Values may be sent and summed in bfloat16 or wider, within the bound.
A program may use at most 64 MiB of HBM per device.

v0:
```python
import functools

import jax
import jax.numpy as jnp
from jax import lax
from jax.experimental import pallas as pl
from jax.experimental.pallas import tpu as pltpu
from jax.sharding import PartitionSpec as P

QK = 128
VD = 256
EPSILON = 1e-06
MESH = pl.DeviceIdType.MESH
F32 = jnp.float32
BF16 = jnp.bfloat16


def dot(a, b):
    return jnp.dot(a, b, preferred_element_type=F32)


def dot_rows(a, b):
    return lax.dot_general(a, b, (((1,), (1,)), ((), ())), preferred_element_type=F32)


def layer_kernel(
    kv_size,
    tp_size,
    tokens_in,
    mix_gain_in,
    w_query,
    w_key,
    w_value,
    w_outgate,
    w_gates,
    forget_bias_in,
    memory,
    normalizer_in,
    stabilizer_in,
    head_gain_in,
    w_out,
    mlp_gain_in,
    w_gate,
    w_up,
    w_down,
    out_mixed,
    vmem,
    out_normalizer,
    out_stabilizer,
    vq,
    vk,
    vv,
    vo,
    vgates,
    tokens,
    mix_gain,
    forget_bias,
    normalizer,
    stabilizer,
    head_gain,
    mlp_gain,
    vwout,
    vgate,
    vup,
    vdown,
    send_qk,
    send_vo,
    send_gs,
    recv_qk,
    recv_vo,
    recv_gs,
    heads_all,
    branch_own,
    branch_recv,
    resid_all,
    gain_rows,
    down_send,
    down_recv,
    load_sem,
    small_sem,
    send1,
    recv1,
    send2,
    recv2,
    send3,
    recv3,
    send4,
    recv4,
    send5,
    recv5,
):
    me = lax.axis_index("kv")
    core = lax.axis_index("tp")
    rows, cols = tokens.shape
    seq = rows // kv_size
    width = cols * kv_size
    local_heads = forget_bias.shape[1]
    total_heads = local_heads * tp_size
    half = local_heads * VD // 2
    group = kv_size * tp_size
    rank = me * tp_size + core
    out_cols = width // group

    loads = [
        pltpu.make_async_copy(src, dst, load_sem.at[i])
        for i, (src, dst) in enumerate(
            (
                (w_gates.at[:, pl.ds(pl.multiple_of(me * cols, cols), cols)], vgates),
                (w_query, vq),
                (w_key, vk),
                (w_value, vv),
                (w_outgate, vo),
                (memory, vmem),
                (w_out, vwout),
                (w_gate, vgate),
                (w_up, vup),
                (w_down, vdown),
            )
        )
    ]
    small = [
        pltpu.make_async_copy(src, dst, small_sem.at[i])
        for i, (src, dst) in enumerate(
            (
                (tokens_in, tokens),
                (mix_gain_in, mix_gain),
                (mlp_gain_in, mlp_gain),
                (forget_bias_in, forget_bias),
                (normalizer_in, normalizer),
                (stabilizer_in, stabilizer),
                (head_gain_in, head_gain),
            )
        )
    ]
    for load in small[:2] + loads[:5] + small[2:]:
        load.start()

    def member(step):
        other = lax.rem(rank + step, group)
        return other, {"kv": other // tp_size, "tp": lax.rem(other, tp_size)}

    barrier = pltpu.get_barrier_semaphore()
    for step in range(1, group):
        _, device = member(step)
        pl.semaphore_signal(barrier, inc=1, device_id=device, device_id_type=MESH)

    def exchange(src, dst, send_sem, recv_sem, device):
        return pltpu.make_async_remote_copy(
            src_ref=src,
            dst_ref=dst,
            send_sem=send_sem,
            recv_sem=recv_sem,
            device_id=device,
            device_id_type=MESH,
        )

    small[0].wait()
    small[1].wait()
    activations = tokens[...].astype(F32)
    square_part = jnp.sum(activations * activations, axis=1, keepdims=True)
    scaled = (activations * mix_gain[...]).astype(BF16)
    def stack_send(target, top, bottom):
        for block in range(kv_size):
            own = slice(block * seq, (block + 1) * seq)
            target[block] = jnp.concatenate([top[own], bottom[own]], axis=0).astype(BF16)

    started = []
    order = sorted(range(1, kv_size), key=lambda d: -min(d, kv_size - d))

    def scatter(buffer, landing, kind):
        copies = {}
        for step in order:
            target = lax.rem(me + step, kv_size)
            copy = exchange(
                buffer.at[target],
                landing.at[step - 1],
                send1.at[kind, step - 1],
                recv1.at[kind, step - 1],
                {"kv": target},
            )
            copy.start()
            copies[step] = copy
            started.append(copy)
        return copies

    loads[0].wait()
    gate_part = dot_rows(scaled, vgates[...])
    for block in range(kv_size):
        own = slice(block * seq, (block + 1) * seq)
        send_gs[block, :, 0 : 2 * total_heads] = gate_part[own]
        send_gs[block, :, 2 * total_heads : 2 * total_heads + 1] = square_part[own]
    loads[1].wait()
    query_part = dot(scaled, vq[...])
    loads[2].wait()
    key_part = dot(scaled, vk[...])
    stack_send(send_qk, query_part, key_part)
    pl.semaphore_wait(barrier, group - 1)
    copies_gs = scatter(send_gs, recv_gs, 0)
    copies_qk = scatter(send_qk, recv_qk, 1)
    loads[3].wait()
    value_part = dot(scaled, vv[...])
    loads[4].wait()
    outgate_part = dot(scaled, vo[...])
    stack_send(send_vo, value_part, outgate_part)
    copies_vo = scatter(send_vo, recv_vo, 2)
    for load in loads[5:]:
        load.start()
    for load in small[2:]:
        load.wait()
    for block in range(kv_size):
        gain_rows[block] = mlp_gain[:, block * cols : (block + 1) * cols]

    def total(buffer, landing, copies):
        result = buffer[me].astype(F32)
        for step in copies:
            copies[step].wait_recv()
            result = result + landing[step - 1].astype(F32)
        return result

    gate_sum = total(send_gs, recv_gs, copies_gs)
    inverse = lax.rsqrt(gate_sum[:, 2 * total_heads : 2 * total_heads + 1] / width + EPSILON)
    gate_pre = gate_sum[:, : 2 * total_heads] * inverse

    def own_columns(start):
        picked = gate_pre[:, start : start + local_heads]
        for other in range(1, tp_size):
            first = start + other * local_heads
            picked = jnp.where(core == other, gate_pre[:, first : first + local_heads], picked)
        return picked

    input_pre = own_columns(0)
    forget_pre = own_columns(total_heads) + forget_bias[...]
    log_forget = jnp.minimum(forget_pre, 0.0) - jnp.log1p(jnp.exp(-jnp.abs(forget_pre)))
    carried_log = log_forget + stabilizer[...].T
    new_stabilizer = jnp.maximum(carried_log, input_pre)
    out_stabilizer[...] = new_stabilizer.T
    forget_scale = jnp.exp(carried_log - new_stabilizer)
    input_scale = jnp.exp(input_pre - new_stabilizer)

    qk_sum = total(send_qk, recv_qk, copies_qk)
    query = (qk_sum[:seq] * inverse).astype(BF16).astype(F32)
    key = (qk_sum[seq:] * (inverse * QK ** (-0.5))).astype(BF16).astype(F32)
    loads[5].wait()
    states = []
    for head in range(local_heads):
        span = slice(head * QK, (head + 1) * QK)
        q, k = query[:, span], key[:, span]
        forget, gain = forget_scale[:, head : head + 1], input_scale[:, head : head + 1]
        scaled_key = gain * k
        new_norm = forget * normalizer[:, head, :] + scaled_key
        out_normalizer[:, head, :] = new_norm
        denominator = jnp.sum(q * new_norm, axis=1, keepdims=True)
        query_key = jnp.sum(q * k, axis=1, keepdims=True)
        q_columns = q.T
        carried = jnp.concatenate(
            [
                jnp.sum(q_columns[:, b : b + 1] * vmem[b, head], axis=0, keepdims=True)
                for b in range(seq)
            ],
            axis=0,
        )
        states.append((forget, gain, scaled_key, denominator, query_key, carried))

    vo_sum = total(send_vo, recv_vo, copies_vo)
    values = (vo_sum[:seq] * inverse).astype(BF16).astype(F32)
    outgate = (vo_sum[seq:] * inverse).astype(BF16).astype(F32)
    mixed = []
    for head in range(local_heads):
        forget, gain, scaled_key, denominator, query_key, carried = states[head]
        span = slice(head * VD, (head + 1) * VD)
        numerator = forget * carried + (gain * query_key) * values[:, span]
        head_out = numerator / jnp.maximum(jnp.abs(denominator), 1.0)
        normed = (
            head_out
            * lax.rsqrt(jnp.mean(head_out * head_out, axis=1, keepdims=True) + EPSILON)
            * head_gain[head : head + 1, :]
        )
        mixed.append(normed * jax.nn.sigmoid(outgate[:, span]))
    mixed = jnp.concatenate(mixed, axis=1)
    heads_all[me] = jnp.concatenate([mixed[:, :half], mixed[:, half:]], axis=0).astype(BF16)

    def spread(buffer, send_sem, recv_sem):
        copies = {}
        for step in order:
            copy = exchange(
                buffer.at[me],
                buffer.at[me],
                send_sem.at[step - 1],
                recv_sem.at[step - 1],
                {"kv": lax.rem(me + step, kv_size)},
            )
            copy.start()
            copies[step] = copy
            started.append(copy)
        return copies

    copies_heads = spread(heads_all, send2, recv2)

    for head in range(local_heads):
        forget, gain, scaled_key, denominator, query_key, carried = states[head]
        k_columns = scaled_key.T
        forget_rows = jnp.broadcast_to(forget, (seq, VD))
        for b in range(seq):
            vmem[b, head] = (
                forget_rows[b : b + 1] * vmem[b, head]
                + k_columns[:, b : b + 1] * values[b : b + 1, head * VD : (head + 1) * VD]
            )

    loads[6].wait()
    for step in copies_heads:
        copies_heads[step].wait_recv()
    gathered = [heads_all[block].astype(F32) for block in range(kv_size)]
    low = jnp.concatenate([g[:seq] for g in gathered], axis=0).astype(BF16)
    high = jnp.concatenate([g[seq:] for g in gathered], axis=0).astype(BF16)
    branch_own[...] = (dot(low, vwout[:half, :]) + dot(high, vwout[half:, :])).astype(BF16)
    copies_branch = []
    for step in range(1, tp_size):
        copy = exchange(
            branch_own,
            branch_recv.at[step - 1],
            send3.at[step - 1],
            recv3.at[step - 1],
            {"tp": lax.rem(core + step, tp_size)},
        )
        copy.start()
        copies_branch.append(copy)
        started.append(copy)
    branch = branch_own[...].astype(F32)
    for step, copy in enumerate(copies_branch):
        copy.wait_recv()
        branch = branch + branch_recv[step].astype(F32)
    residual = (activations + branch).astype(BF16)
    resid_all[me] = residual
    copies_resid = spread(resid_all, send4, recv4)

    loads[7].wait()
    loads[8].wait()
    gate_value = up_value = square_sum = 0.0
    for step in [0] + order[::-1]:
        source = lax.rem(me - step + kv_size, kv_size)
        if step:
            copies_resid[step].wait_recv()
        block = resid_all[source].astype(F32)
        square_sum = square_sum + jnp.sum(block * block, axis=1, keepdims=True)
        block = (block * gain_rows[source]).astype(BF16)
        span = pl.ds(pl.multiple_of(source * cols, cols), cols)
        gate_value = gate_value + dot_rows(block, vgate[:, span])
        up_value = up_value + dot_rows(block, vup[:, span])
    inverse_two = lax.rsqrt(square_sum / width + EPSILON)
    gate_value = gate_value * inverse_two
    up_value = up_value * inverse_two
    hidden = (gate_value * jax.nn.sigmoid(gate_value) * up_value).astype(BF16)

    loads[9].wait()
    dynamic = out_cols % 128 == 0
    if not dynamic:
        for block in range(group):
            down_send[block] = dot(
                hidden, vdown[:, block * out_cols : (block + 1) * out_cols]
            ).astype(BF16)

    def down_block(block):
        if dynamic:
            span = pl.ds(pl.multiple_of(block * out_cols, out_cols), out_cols)
            return dot(hidden, vdown[:, span])
        return down_send[block].astype(F32)

    def distance(step):
        away = -(-step // tp_size)
        return min(away, kv_size - away)

    copies_down = {}
    for step in sorted(range(1, group), key=lambda s: -distance(s)):
        block, device = member(step)
        if dynamic:
            down_send[block] = down_block(block).astype(BF16)
        copy = exchange(
            down_send.at[block],
            down_recv.at[step - 1],
            send5.at[step - 1],
            recv5.at[step - 1],
            device,
        )
        copy.start()
        copies_down[step] = copy
        started.append(copy)
    summed = down_block(rank)
    own_residual = residual[:, :out_cols].astype(F32)
    for other in range(1, tp_size):
        own_residual = jnp.where(
            core == other,
            residual[:, other * out_cols : (other + 1) * out_cols].astype(F32),
            own_residual,
        )
    for step in sorted(copies_down, key=distance):
        copies_down[step].wait_recv()
        summed = summed + down_recv[step - 1].astype(F32)
    out_mixed[...] = (summed + own_residual).astype(BF16)
    for copy in started:
        copy.wait_send()


def store_kernel(mixed, memory, normalizer, stabilizer, *rest):
    sem = rest[-1]
    copies = [
        pltpu.make_async_copy(src, dst, sem.at[i])
        for i, (src, dst) in enumerate(zip((mixed, memory, normalizer, stabilizer), rest))
    ]
    for copy in copies:
        copy.start()
    for copy in copies:
        copy.wait()


def body(kv_size, tp_size, *args):
    (
        tokens,
        mix_gain,
        w_query,
        w_key,
        w_value,
        w_outgate,
        w_gates,
        forget_bias,
        memory,
        normalizer,
        stabilizer,
        head_gain,
        w_out,
        mlp_gain,
        w_gate,
        w_up,
        w_down,
    ) = args
    w_gates, w_gate, w_up, stabilizer = w_gates.T, w_gate.T, w_up.T, stabilizer.T
    rows, cols = tokens.shape
    local_heads, seq = stabilizer.shape
    group = kv_size * tp_size
    out_cols = cols // tp_size
    half = local_heads * VD // 2
    vmem = pl.BlockSpec(memory_space=pltpu.VMEM)
    hbm = pl.BlockSpec(memory_space=pl.ANY)
    peers = kv_size - 1

    def like(array):
        return pltpu.VMEM(array.shape, array.dtype)

    results = (
        ((rows, out_cols), BF16),
        (memory.shape, F32),
        (normalizer.shape, F32),
        (stabilizer.shape, F32),
    )
    gains = (mix_gain.reshape(1, cols), mlp_gain.reshape(1, mlp_gain.shape[0]))
    forget_bias = forget_bias.reshape(1, local_heads)
    held = pl.pallas_call(
        functools.partial(layer_kernel, kv_size, tp_size),
        out_shape=tuple(pltpu.VMEM(*result) for result in results),
        in_specs=[hbm] * len(args),
        out_specs=(vmem,) * len(results),
        scratch_shapes=[
            like(w_query),
            like(w_key),
            like(w_value),
            like(w_outgate),
            pltpu.VMEM((w_gates.shape[0], cols), BF16),
            like(tokens),
            like(gains[0]),
            like(forget_bias),
            like(normalizer),
            like(stabilizer),
            like(head_gain),
            like(gains[1]),
            like(w_out),
            like(w_gate),
            like(w_up),
            like(w_down),
            pltpu.VMEM((kv_size, 2 * seq, local_heads * QK), BF16),
            pltpu.VMEM((kv_size, 2 * seq, local_heads * VD), BF16),
            pltpu.VMEM((kv_size, seq, 128), F32),
            pltpu.VMEM((peers, 2 * seq, local_heads * QK), BF16),
            pltpu.VMEM((peers, 2 * seq, local_heads * VD), BF16),
            pltpu.VMEM((peers, seq, 128), F32),
            pltpu.VMEM((kv_size, 2 * seq, half), BF16),
            pltpu.VMEM((rows, cols), BF16),
            pltpu.VMEM((tp_size - 1, rows, cols), BF16),
            pltpu.VMEM((kv_size, rows, cols), BF16),
            pltpu.VMEM((kv_size, 1, cols), F32),
            pltpu.VMEM((group, rows, out_cols), BF16),
            pltpu.VMEM((group - 1, rows, out_cols), BF16),
            pltpu.SemaphoreType.DMA((10,)),
            pltpu.SemaphoreType.DMA((7,)),
            pltpu.SemaphoreType.DMA((3, peers)),
            pltpu.SemaphoreType.DMA((3, peers)),
            pltpu.SemaphoreType.DMA((peers,)),
            pltpu.SemaphoreType.DMA((peers,)),
            pltpu.SemaphoreType.DMA((tp_size - 1,)),
            pltpu.SemaphoreType.DMA((tp_size - 1,)),
            pltpu.SemaphoreType.DMA((peers,)),
            pltpu.SemaphoreType.DMA((peers,)),
            pltpu.SemaphoreType.DMA((group - 1,)),
            pltpu.SemaphoreType.DMA((group - 1,)),
        ],
        compiler_params=pltpu.CompilerParams(
            collective_id=0, has_side_effects=True, vmem_limit_bytes=48 * 2**20
        ),
    )(*(pltpu.with_memory_space_constraint(x, pltpu.HBM) for x in (
        tokens,
        gains[0],
        w_query,
        w_key,
        w_value,
        w_outgate,
        w_gates,
        forget_bias,
        memory,
        normalizer,
        stabilizer,
        head_gain,
        w_out,
        gains[1],
        w_gate,
        w_up,
        w_down,
    )))
    mixed_out, new_memory, new_normalizer, new_stabilizer = pl.pallas_call(
        store_kernel,
        out_shape=tuple(jax.ShapeDtypeStruct(*result) for result in results),
        in_specs=[vmem] * len(results),
        out_specs=(hbm,) * len(results),
        scratch_shapes=[pltpu.SemaphoreType.DMA((len(results),))],
        compiler_params=pltpu.CompilerParams(vmem_limit_bytes=2**20),
    )(*held)
    return mixed_out, new_memory, new_normalizer, new_stabilizer.T


def solution(mesh):
    in_specs = (
        P("dp", "kv"),
        P("kv"),
        P("kv", "tp"),
        P("kv", "tp"),
        P("kv", "tp"),
        P("kv", "tp"),
        P(),
        P("tp"),
        P(("dp", "kv"), "tp", None, None),
        P(("dp", "kv"), "tp", None),
        P(("dp", "kv"), "tp"),
        P("tp", None),
        P("tp", "kv"),
        P(),
        P(None, ("kv", "tp")),
        P(None, ("kv", "tp")),
        P(("kv", "tp"), None),
    )
    out_specs = (
        P("dp", ("kv", "tp")),
        P(("dp", "kv"), "tp", None, None),
        P(("dp", "kv"), "tp", None),
        P(("dp", "kv"), "tp"),
    )
    return jax.shard_map(
        functools.partial(body, mesh.shape["kv"], mesh.shape["tp"]),
        mesh=mesh,
        in_specs=in_specs,
        out_specs=out_specs,
        check_vma=False,
    )
```

profile of v0, /device:TPU:0, one launch (start us, length us, event | category | flops | bytes accessed | tf_op | source)
XLA Modules:
  0.0 30.9 jit_solution(16121766867759774867)
XLA Ops:
  0.6 28.1 %shard_map.192 = (bf16[32,256]{1,0:T(8,128)(2,1)S(1)}, f32[8,4,128,256]{3,2,1,0:T(8,128)S(1)}, f32[8,4,128]{2,1,0:T(4,128)S(1)}, f32[4,8]{1,0:T(4,128)S(1)}) custom-call(bf16[32,512]{1,0:T(8,128)(2,1)} %tokens_in.1, f32[1,512]{1,0:T(1,128)} %bitcast.12, bf16[512,512]{1,0:T(8,128)(2,1)} %w_query.1, bf16[512,512]{1,0:T(8,128)(2,1)} %w_key.1, ...), custom_call_target="tpu_custom_call" | custom-call | tf_op jit(solution)/shard_map/pallas_call | solution.py:456
  28.8 2.1 %shard_map.193 = (bf16[32,256]{1,0:T(8,128)(2,1)}, f32[8,4,128,256]{3,2,1,0:T(8,128)}, f32[8,4,128]{2,1,0:T(4,128)}, f32[4,8]{1,0:T(4,128)}) custom-call(bf16[32,256]{1,0:T(8,128)(2,1)S(1)} %get-tuple-element.12.mixed, f32[8,4,128,256]{3,2,1,0:T(8,128)S(1)} %get-tuple-element.13.memory, f32[8,4,128]{2,1,0:T(4,128)S(1)} %get-tuple-element.14.normalizer, ...), custom_call_target="tpu_custom_call" | custom-call | tf_op jit(solution)/shard_map/pallas_call | solution.py:526
where the time goes:
time: 31 us; the launch traced here: 30.9 us
  Pallas kernels  30.2 us (97%)
  between operations  0.65 us (2%)
    pallas_call x1, Pallas kernels, body(): pl.pallas_call(functools.partial(layer_kernel, kv_size, tp_size), out_sha...  28.1 us
    pallas_call x1, Pallas kernels, body(): pl.pallas_call(store_kernel, out_shape=tuple((jax.ShapeDtypeStruct(*resul...  2.06 us

commit v1 on v0

--- a/solution.py
+++ b/solution.py
@@ -21,6 +21,13 @@
 
 def dot_rows(a, b):
     return lax.dot_general(a, b, (((1,), (1,)), ((), ())), preferred_element_type=F32)
+
+
+def nearest(rank, me, size):
+    inner = jnp.minimum(me, size - 1 - me)
+    close = me + ((rank + 1) // 2 if rank % 2 else -(rank // 2))
+    beyond = (rank - inner) * jnp.where(2 * me < size - 1, 1, -1)
+    return jnp.where(rank <= 2 * inner, close, me + beyond)
 
 
 def layer_kernel(
@@ -74,19 +81,18 @@
     branch_recv,
     resid_all,
     gain_rows,
+    down_pair,
+    pair_recv,
     down_send,
     down_recv,
     load_sem,
     small_sem,
-    send1,
+    send_sem,
     recv1,
-    send2,
     recv2,
-    send3,
     recv3,
-    send4,
     recv4,
-    send5,
+    pair_sem,
     recv5,
 ):
     me = lax.axis_index("kv")
@@ -98,8 +104,22 @@
     total_heads = local_heads * tp_size
     half = local_heads * VD // 2
     group = kv_size * tp_size
+    out_cols = width // group
+    chunks = pair_recv.shape[1]
+    chunk_chips = kv_size // chunks
+    chunk_cols = width // chunks
+    last = tp_size - 1
+
+    barrier = pltpu.get_barrier_semaphore()
     rank = me * tp_size + core
-    out_cols = width // group
+    for step in range(1, group):
+        other = lax.rem(rank + step, group)
+        pl.semaphore_signal(
+            barrier,
+            inc=1,
+            device_id={"kv": other // tp_size, "tp": lax.rem(other, tp_size)},
+            device_id_type=MESH,
+        )
 
     loads = [
         pltpu.make_async_copy(src, dst, load_sem.at[i])
@@ -135,53 +155,36 @@
     for load in small[:2] + loads[:5] + small[2:]:
         load.start()
 
-    def member(step):
-        other = lax.rem(rank + step, group)
-        return other, {"kv": other // tp_size, "tp": lax.rem(other, tp_size)}
-
-    barrier = pltpu.get_barrier_semaphore()
-    for step in range(1, group):
-        _, device = member(step)
-        pl.semaphore_signal(barrier, inc=1, device_id=device, device_id_type=MESH)
-
-    def exchange(src, dst, send_sem, recv_sem, device):
-        return pltpu.make_async_remote_copy(
+    def send(src, dst, index, recv_sem, device):
+        pltpu.make_async_remote_copy(
             src_ref=src,
             dst_ref=dst,
-            send_sem=send_sem,
+            send_sem=send_sem.at[index],
             recv_sem=recv_sem,
             device_id=device,
             device_id_type=MESH,
-        )
+        ).start()
+
+    def drain(ref, sem):
+        pltpu.make_async_copy(ref, ref, sem).wait()
+
+    far_first = [nearest(k, me, kv_size) for k in range(kv_size - 1, 0, -1)]
+    near_first = far_first[::-1]
 
     small[0].wait()
     small[1].wait()
     activations = tokens[...].astype(F32)
     square_part = jnp.sum(activations * activations, axis=1, keepdims=True)
     scaled = (activations * mix_gain[...]).astype(BF16)
+
     def stack_send(target, top, bottom):
         for block in range(kv_size):
             own = slice(block * seq, (block + 1) * seq)
             target[block] = jnp.concatenate([top[own], bottom[own]], axis=0).astype(BF16)
 
-    started = []
-    order = sorted(range(1, kv_size), key=lambda d: -min(d, kv_size - d))
-
     def scatter(buffer, landing, kind):
-        copies = {}
-        for step in order:
-            target = lax.rem(me + step, kv_size)
-            copy = exchange(
-                buffer.at[target],
-                landing.at[step - 1],
-                send1.at[kind, step - 1],
-                recv1.at[kind, step - 1],
-                {"kv": target},
-            )
-            copy.start()
-            copies[step] = copy
-            started.append(copy)
-        return copies
+        for target in far_first:
+            send(buffer.at[target], landing.at[me], kind, recv1.at[kind, me], {"kv": target})
 
     loads[0].wait()
     gate_part = dot_rows(scaled, vgates[...])
@@ -195,14 +198,21 @@
     key_part = dot(scaled, vk[...])
     stack_send(send_qk, query_part, key_part)
     pl.semaphore_wait(barrier, group - 1)
-    copies_gs = scatter(send_gs, recv_gs, 0)
-    copies_qk = scatter(send_qk, recv_qk, 1)
+    scatter(send_gs, recv_gs, 0)
+    scatter(send_qk, recv_qk, 1)
     loads[3].wait()
     value_part = dot(scaled, vv[...])
     loads[4].wait()
     outgate_part = dot(scaled, vo[...])
     stack_send(send_vo, value_part, outgate_part)
-    copies_vo = scatter(send_vo, recv_vo, 2)
+
+    def send_values():
+        scatter(send_vo, recv_vo, 2)
+
+    @pl.when(core == 0)
+    def _():
+        send_values()
+
     for load in loads[5:]:
         load.start()
     for load in small[2:]:
@@ -210,14 +220,19 @@
     for block in range(kv_size):
         gain_rows[block] = mlp_gain[:, block * cols : (block + 1) * cols]
 
-    def total(buffer, landing, copies):
+    def total(buffer, landing, kind):
         result = buffer[me].astype(F32)
-        for step in copies:
-            copies[step].wait_recv()
-            result = result + landing[step - 1].astype(F32)
+        for source in near_first:
+            drain(landing.at[source], recv1.at[kind, source])
+            result = result + landing[source].astype(F32)
         return result
 
-    gate_sum = total(send_gs, recv_gs, copies_gs)
+    gate_sum = total(send_gs, recv_gs, 0)
+
+    @pl.when(core != 0)
+    def _():
+        send_values()
+
     inverse = lax.rsqrt(gate_sum[:, 2 * total_heads : 2 * total_heads + 1] / width + EPSILON)
     gate_pre = gate_sum[:, : 2 * total_heads] * inverse
 
@@ -237,7 +252,7 @@
     forget_scale = jnp.exp(carried_log - new_stabilizer)
     input_scale = jnp.exp(input_pre - new_stabilizer)
 
-    qk_sum = total(send_qk, recv_qk, copies_qk)
+    qk_sum = total(send_qk, recv_qk, 1)
     query = (qk_sum[:seq] * inverse).astype(BF16).astype(F32)
     key = (qk_sum[seq:] * (inverse * QK ** (-0.5))).astype(BF16).astype(F32)
     loads[5].wait()
@@ -261,7 +276,7 @@
         )
         states.append((forget, gain, scaled_key, denominator, query_key, carried))
 
-    vo_sum = total(send_vo, recv_vo, copies_vo)
+    vo_sum = total(send_vo, recv_vo, 2)
     values = (vo_sum[:seq] * inverse).astype(BF16).astype(F32)
     outgate = (vo_sum[seq:] * inverse).astype(BF16).astype(F32)
     mixed = []
@@ -278,23 +293,8 @@
         mixed.append(normed * jax.nn.sigmoid(outgate[:, span]))
     mixed = jnp.concatenate(mixed, axis=1)
     heads_all[me] = jnp.concatenate([mixed[:, :half], mixed[:, half:]], axis=0).astype(BF16)
-
-    def spread(buffer, send_sem, recv_sem):
-        copies = {}
-        for step in order:
-            copy = exchange(
-                buffer.at[me],
-                buffer.at[me],
-                send_sem.at[step - 1],
-                recv_sem.at[step - 1],
-                {"kv": lax.rem(me + step, kv_size)},
-            )
-            copy.start()
-            copies[step] = copy
-            started.append(copy)
-        return copies
-
-    copies_heads = spread(heads_all, send2, recv2)
+    for target in far_first:
+        send(heads_all.at[me], heads_all.at[me], 3, recv2.at[me], {"kv": target})
 
     for head in range(local_heads):
         forget, gain, scaled_key, denominator, query_key, carried = states[head]
@@ -307,39 +307,51 @@
             )
 
     loads[6].wait()
-    for step in copies_heads:
-        copies_heads[step].wait_recv()
+    for source in near_first:
+        drain(heads_all.at[source], recv2.at[source])
     gathered = [heads_all[block].astype(F32) for block in range(kv_size)]
     low = jnp.concatenate([g[:seq] for g in gathered], axis=0).astype(BF16)
     high = jnp.concatenate([g[seq:] for g in gathered], axis=0).astype(BF16)
     branch_own[...] = (dot(low, vwout[:half, :]) + dot(high, vwout[half:, :])).astype(BF16)
-    copies_branch = []
-    for step in range(1, tp_size):
-        copy = exchange(
-            branch_own,
-            branch_recv.at[step - 1],
-            send3.at[step - 1],
-            recv3.at[step - 1],
-            {"tp": lax.rem(core + step, tp_size)},
-        )
-        copy.start()
-        copies_branch.append(copy)
-        started.append(copy)
-    branch = branch_own[...].astype(F32)
-    for step, copy in enumerate(copies_branch):
-        copy.wait_recv()
-        branch = branch + branch_recv[step].astype(F32)
-    residual = (activations + branch).astype(BF16)
-    resid_all[me] = residual
-    copies_resid = spread(resid_all, send4, recv4)
+
+    @pl.when(core != 0)
+    def _():
+        send(branch_own, branch_recv.at[core - 1], 4, recv3.at[core - 1], {"tp": 0})
+
+    @pl.when(core == 0)
+    def _():
+        branch = branch_own[...].astype(F32)
+        for other in range(tp_size - 1):
+            drain(branch_recv.at[other], recv3.at[other])
+            branch = branch + branch_recv[other].astype(F32)
+        resid_all[me] = (activations + branch).astype(BF16)
+        for target in far_first:
+            send(resid_all.at[me], resid_all.at[me], 4, recv4.at[me], {"kv": target})
+
+    def pass_on(source):
+        for other in range(1, tp_size):
+            send(
+                resid_all.at[source],
+                resid_all.at[source],
+                5,
+                recv4.at[source],
+                {"tp": other},
+            )
 
     loads[7].wait()
     loads[8].wait()
     gate_value = up_value = square_sum = 0.0
-    for step in [0] + order[::-1]:
-        source = lax.rem(me - step + kv_size, kv_size)
-        if step:
-            copies_resid[step].wait_recv()
+    for source in [me] + near_first:
+        @pl.when(core == 0)
+        def _():
+            if source is not me:
+                drain(resid_all.at[source], recv4.at[source])
+            pass_on(source)
+
+        @pl.when(core != 0)
+        def _():
+            drain(resid_all.at[source], recv4.at[source])
+
         block = resid_all[source].astype(F32)
         square_sum = square_sum + jnp.sum(block * block, axis=1, keepdims=True)
         block = (block * gain_rows[source]).astype(BF16)
@@ -352,52 +364,99 @@
     hidden = (gate_value * jax.nn.sigmoid(gate_value) * up_value).astype(BF16)
 
     loads[9].wait()
-    dynamic = out_cols % 128 == 0
-    if not dynamic:
-        for block in range(group):
-            down_send[block] = dot(
-                hidden, vdown[:, block * out_cols : (block + 1) * out_cols]
-            ).astype(BF16)
-
-    def down_block(block):
-        if dynamic:
-            span = pl.ds(pl.multiple_of(block * out_cols, out_cols), out_cols)
-            return dot(hidden, vdown[:, span])
-        return down_send[block].astype(F32)
-
-    def distance(step):
-        away = -(-step // tp_size)
-        return min(away, kv_size - away)
-
-    copies_down = {}
-    for step in sorted(range(1, group), key=lambda s: -distance(s)):
-        block, device = member(step)
-        if dynamic:
-            down_send[block] = down_block(block).astype(BF16)
-        copy = exchange(
-            down_send.at[block],
-            down_recv.at[step - 1],
-            send5.at[step - 1],
-            recv5.at[step - 1],
-            device,
-        )
-        copy.start()
-        copies_down[step] = copy
-        started.append(copy)
-    summed = down_block(rank)
-    own_residual = residual[:, :out_cols].astype(F32)
-    for other in range(1, tp_size):
-        own_residual = jnp.where(
-            core == other,
-            residual[:, other * out_cols : (other + 1) * out_cols].astype(F32),
-            own_residual,
-        )
-    for step in sorted(copies_down, key=distance):
-        copies_down[step].wait_recv()
-        summed = summed + down_recv[step - 1].astype(F32)
-    out_mixed[...] = (summed + own_residual).astype(BF16)
-    for copy in started:
-        copy.wait_send()
+    upper = me >= kv_size // 2
+    for step in range(chunks):
+        chunk = jnp.where(upper, step, chunks - 1 - step) if chunks > 1 else 0
+        span = pl.ds(pl.multiple_of(chunk * chunk_cols, chunk_cols), chunk_cols)
+        part = dot(hidden, vdown[:, span])
+
+        @pl.when(core != last)
+        def _():
+            down_pair[step] = part.astype(BF16)
+            send(
+                down_pair.at[step],
+                pair_recv.at[core, step],
+                6,
+                pair_sem.at[core, step],
+                {"tp": last},
+            )
+
+        @pl.when(core == last)
+        def _():
+            summed = part
+            for other in range(last):
+                drain(pair_recv.at[other, step], pair_sem.at[other, step])
+                summed = summed + pair_recv[other, step].astype(F32)
+            for chip in range(chunk_chips):
+                for other in range(tp_size):
+                    index = (chunk * chunk_chips + chip) * tp_size + other
+                    first = (chip * tp_size + other) * out_cols
+                    down_send[index] = summed[:, first : first + out_cols].astype(BF16)
+            base = chunk * chunk_chips
+            for place in range(chunk_chips):
+                chip = base + jnp.where(upper, place, chunk_chips - 1 - place)
+                for other in range(tp_size):
+                    block = down_send.at[chip * tp_size + other]
+
+                    @pl.when(chip != me)
+                    def _():
+                        send(
+                            block,
+                            down_recv.at[me],
+                            6,
+                            recv5.at[me],
+                            {"kv": chip, "tp": other},
+                        )
+
+                    if other != last:
+                        @pl.when(chip == me)
+                        def _():
+                            send(block, down_recv.at[me], 6, recv5.at[me], {"tp": other})
+
+    @pl.when(core == last)
+    def _():
+        down_recv[me] = down_send[me * tp_size + last]
+
+    @pl.when(core != last)
+    def _():
+        drain(down_recv.at[me], recv5.at[me])
+
+    residual = resid_all[me].astype(F32)
+    summed = down_recv[me].astype(F32) + residual[:, :out_cols]
+    if tp_size > 1:
+        own_residual = residual[:, :out_cols]
+        for other in range(1, tp_size):
+            own_residual = jnp.where(
+                core == other, residual[:, other * out_cols : (other + 1) * out_cols], own_residual
+            )
+        summed = down_recv[me].astype(F32) + own_residual
+    for source in near_first:
+        drain(down_recv.at[source], recv5.at[source])
+        summed = summed + down_recv[source].astype(F32)
+    out_mixed[...] = summed.astype(BF16)
+    peers = kv_size - 1
+    drain(send_gs.at[:peers], send_sem.at[0])
+    drain(send_qk.at[:peers], send_sem.at[1])
+    drain(send_vo.at[:peers], send_sem.at[2])
+    drain(heads_all.at[:peers], send_sem.at[3])
+
+    @pl.when(core == 0)
+    def _():
+        drain(resid_all.at[:peers], send_sem.at[4])
+        for _ in range(tp_size - 1):
+            drain(resid_all, send_sem.at[5])
+
+    @pl.when(core != 0)
+    def _():
+        drain(branch_own, send_sem.at[4])
+
+    @pl.when(core == last)
+    def _():
+        drain(down_send.at[: group - 1], send_sem.at[6])
+
+    @pl.when(core != last)
+    def _():
+        drain(down_pair, send_sem.at[6])
 
 
 def store_kernel(mixed, memory, normalizer, stabilizer, *rest):
@@ -440,7 +499,8 @@
     half = local_heads * VD // 2
     vmem = pl.BlockSpec(memory_space=pltpu.VMEM)
     hbm = pl.BlockSpec(memory_space=pl.ANY)
-    peers = kv_size - 1
+    width = cols * kv_size
+    chunks = 2 if kv_size % 2 == 0 else 1
 
     def like(array):
         return pltpu.VMEM(array.shape, array.dtype)
@@ -478,28 +538,27 @@
             pltpu.VMEM((kv_size, 2 * seq, local_heads * QK), BF16),
             pltpu.VMEM((kv_size, 2 * seq, local_heads * VD), BF16),
             pltpu.VMEM((kv_size, seq, 128), F32),
-            pltpu.VMEM((peers, 2 * seq, local_heads * QK), BF16),
-            pltpu.VMEM((peers, 2 * seq, local_heads * VD), BF16),
-            pltpu.VMEM((peers, seq, 128), F32),
+            pltpu.VMEM((kv_size, 2 * seq, local_heads * QK), BF16),
+            pltpu.VMEM((kv_size, 2 * seq, local_heads * VD), BF16),
+            pltpu.VMEM((kv_size, seq, 128), F32),
             pltpu.VMEM((kv_size, 2 * seq, half), BF16),
             pltpu.VMEM((rows, cols), BF16),
-            pltpu.VMEM((tp_size - 1, rows, cols), BF16),
+            pltpu.VMEM((max(tp_size - 1, 1), rows, cols), BF16),
             pltpu.VMEM((kv_size, rows, cols), BF16),
             pltpu.VMEM((kv_size, 1, cols), F32),
+            pltpu.VMEM((chunks, rows, width // chunks), BF16),
+            pltpu.VMEM((max(tp_size - 1, 1), chunks, rows, width // chunks), BF16),
             pltpu.VMEM((group, rows, out_cols), BF16),
-            pltpu.VMEM((group - 1, rows, out_cols), BF16),
+            pltpu.VMEM((kv_size, rows, out_cols), BF16),
             pltpu.SemaphoreType.DMA((10,)),
             pltpu.SemaphoreType.DMA((7,)),
-            pltpu.SemaphoreType.DMA((3, peers)),
-            pltpu.SemaphoreType.DMA((3, peers)),
-            pltpu.SemaphoreType.DMA((peers,)),
-            pltpu.SemaphoreType.DMA((peers,)),
-            pltpu.SemaphoreType.DMA((tp_size - 1,)),
-            pltpu.SemaphoreType.DMA((tp_size - 1,)),
-            pltpu.SemaphoreType.DMA((peers,)),
-            pltpu.SemaphoreType.DMA((peers,)),
-            pltpu.SemaphoreType.DMA((group - 1,)),
-            pltpu.SemaphoreType.DMA((group - 1,)),
+            pltpu.SemaphoreType.DMA((7,)),
+            pltpu.SemaphoreType.DMA((3, kv_size)),
+            pltpu.SemaphoreType.DMA((kv_size,)),
+            pltpu.SemaphoreType.DMA((max(tp_size - 1, 1),)),
+            pltpu.SemaphoreType.DMA((kv_size,)),
+            pltpu.SemaphoreType.DMA((max(tp_size - 1, 1), chunks)),
+            pltpu.SemaphoreType.DMA((kv_size,)),
         ],
         compiler_params=pltpu.CompilerParams(
             collective_id=0, has_side_effects=True, vmem_limit_bytes=48 * 2**20

time: 31 us -> 28.6 us (0.923)
  Pallas kernels: 30.2 us -> 27.8 us
    pallas_call x1, Pallas kernels: 28.1 us -> 25.7 us  [body(): pl.pallas_call(functools.partial(layer_kernel, kv_size, tp_size), out_sha...]
where the time goes in v1:
time: 28.6 us; the launch traced here: 28.4 us
  Pallas kernels  27.8 us (97%)
  between operations  0.65 us (2%)
    pallas_call x1, Pallas kernels, body(): pl.pallas_call(functools.partial(layer_kernel, kv_size, tp_size), out_sha...  25.7 us
    pallas_call x1, Pallas kernels, body(): pl.pallas_call(store_kernel, out_shape=tuple((jax.ShapeDtypeStruct(*resul...  2.06 us

profile of v1, /device:TPU:0, one launch (start us, length us, event | category | flops | bytes accessed | tf_op | source)
XLA Modules:
  0.0 28.4 jit_solution(3462490181325809620)
XLA Ops:
  0.6 25.7 %shard_map.192 = (bf16[32,256]{1,0:T(8,128)(2,1)S(1)}, f32[8,4,128,256]{3,2,1,0:T(8,128)S(1)}, f32[8,4,128]{2,1,0:T(4,128)S(1)}, f32[4,8]{1,0:T(4,128)S(1)}) custom-call(bf16[32,512]{1,0:T(8,128)(2,1)} %tokens_in.1, f32[1,512]{1,0:T(1,128)} %bitcast.12, bf16[512,512]{1,0:T(8,128)(2,1)} %w_query.1, bf16[512,512]{1,0:T(8,128)(2,1)} %w_key.1, ...), custom_call_target="tpu_custom_call" | custom-call | tf_op jit(solution)/shard_map/pallas_call | solution.py:516
  26.4 2.1 %shard_map.193 = (bf16[32,256]{1,0:T(8,128)(2,1)}, f32[8,4,128,256]{3,2,1,0:T(8,128)}, f32[8,4,128]{2,1,0:T(4,128)}, f32[4,8]{1,0:T(4,128)}) custom-call(bf16[32,256]{1,0:T(8,128)(2,1)S(1)} %get-tuple-element.12.mixed, f32[8,4,128,256]{3,2,1,0:T(8,128)S(1)} %get-tuple-element.13.memory, f32[8,4,128]{2,1,0:T(4,128)S(1)} %get-tuple-element.14.normalizer, ...), custom_call_target="tpu_custom_call" | custom-call | tf_op jit(solution)/shard_map/pallas_call | solution.py:585

commit v2 on v1

--- a/solution.py
+++ b/solution.py
@@ -9,6 +9,7 @@
 
 QK = 128
 VD = 256
+LANES = 128
 EPSILON = 1e-06
 MESH = pl.DeviceIdType.MESH
 F32 = jnp.float32
@@ -25,9 +26,9 @@
 
 def nearest(rank, me, size):
     inner = jnp.minimum(me, size - 1 - me)
-    close = me + ((rank + 1) // 2 if rank % 2 else -(rank // 2))
-    beyond = (rank - inner) * jnp.where(2 * me < size - 1, 1, -1)
-    return jnp.where(rank <= 2 * inner, close, me + beyond)
+    away = rank // 2 + 1 if rank % 2 else -(rank // 2)
+    away = jnp.where(rank <= 2 * inner, away, rank - inner)
+    return jnp.where(2 * me < size - 1, me + away, me - away)
 
 
 def layer_kernel(
@@ -81,6 +82,8 @@
     branch_recv,
     resid_all,
     gain_rows,
+    gate_sum_ref,
+    up_sum_ref,
     down_pair,
     pair_recv,
     down_send,
@@ -105,10 +108,12 @@
     half = local_heads * VD // 2
     group = kv_size * tp_size
     out_cols = width // group
-    chunks = pair_recv.shape[1]
-    chunk_chips = kv_size // chunks
-    chunk_cols = width // chunks
-    last = tp_size - 1
+    lead = tp_size - 1
+    sink = 0
+    beside_lead = [(lead + 1 + i) % tp_size for i in range(tp_size - 1)]
+    beside_sink = [(sink + 1 + i) % tp_size for i in range(tp_size - 1)]
+    after_lead = lax.rem(core + tp_size - lead - 1 + tp_size, tp_size)
+    after_sink = lax.rem(core + tp_size - sink - 1 + tp_size, tp_size)
 
     barrier = pltpu.get_barrier_semaphore()
     rank = me * tp_size + core
@@ -165,11 +170,16 @@
             device_id_type=MESH,
         ).start()
 
+    def slot(source, target):
+        return lax.rem(source - target + kv_size, kv_size) - 1
+
     def drain(ref, sem):
         pltpu.make_async_copy(ref, ref, sem).wait()
 
     far_first = [nearest(k, me, kv_size) for k in range(kv_size - 1, 0, -1)]
     near_first = far_first[::-1]
+    outer = jnp.minimum(me, kv_size - 1 - me) < kv_size // 4
+    ends_far_first = [jnp.where(outer, a, b) for a, b in zip(far_first, near_first)]
 
     small[0].wait()
     small[1].wait()
@@ -184,7 +194,7 @@
 
     def scatter(buffer, landing, kind):
         for target in far_first:
-            send(buffer.at[target], landing.at[me], kind, recv1.at[kind, me], {"kv": target})
+            send(buffer.at[target], landing.at[me], kind, recv1.at[kind, slot(me, target)], {"kv": target})
 
     loads[0].wait()
     gate_part = dot_rows(scaled, vgates[...])
@@ -199,19 +209,20 @@
     stack_send(send_qk, query_part, key_part)
     pl.semaphore_wait(barrier, group - 1)
     scatter(send_gs, recv_gs, 0)
-    scatter(send_qk, recv_qk, 1)
+
+    @pl.when(core == 0)
+    def _():
+        scatter(send_qk, recv_qk, 1)
+
     loads[3].wait()
     value_part = dot(scaled, vv[...])
     loads[4].wait()
     outgate_part = dot(scaled, vo[...])
     stack_send(send_vo, value_part, outgate_part)
 
-    def send_values():
+    @pl.when(core == 0)
+    def _():
         scatter(send_vo, recv_vo, 2)
-
-    @pl.when(core == 0)
-    def _():
-        send_values()
 
     for load in loads[5:]:
         load.start()
@@ -223,15 +234,11 @@
     def total(buffer, landing, kind):
         result = buffer[me].astype(F32)
         for source in near_first:
-            drain(landing.at[source], recv1.at[kind, source])
+            drain(landing.at[source], recv1.at[kind, slot(source, me)])
             result = result + landing[source].astype(F32)
         return result
 
     gate_sum = total(send_gs, recv_gs, 0)
-
-    @pl.when(core != 0)
-    def _():
-        send_values()
 
     inverse = lax.rsqrt(gate_sum[:, 2 * total_heads : 2 * total_heads + 1] / width + EPSILON)
     gate_pre = gate_sum[:, : 2 * total_heads] * inverse
@@ -252,10 +259,19 @@
     forget_scale = jnp.exp(carried_log - new_stabilizer)
     input_scale = jnp.exp(input_pre - new_stabilizer)
 
+    @pl.when(core != 0)
+    def _():
+        scatter(send_qk, recv_qk, 1)
+        scatter(send_vo, recv_vo, 2)
+
     qk_sum = total(send_qk, recv_qk, 1)
     query = (qk_sum[:seq] * inverse).astype(BF16).astype(F32)
     key = (qk_sum[seq:] * (inverse * QK ** (-0.5))).astype(BF16).astype(F32)
     loads[5].wait()
+    place = lax.broadcasted_iota(jnp.int32, (seq, seq * LANES), 1) // LANES
+    spread = jnp.where(
+        place == lax.broadcasted_iota(jnp.int32, (seq, seq * LANES), 0), 1.0, 0.0
+    ).astype(BF16)
     states = []
     for head in range(local_heads):
         span = slice(head * QK, (head + 1) * QK)
@@ -266,10 +282,21 @@
         out_normalizer[:, head, :] = new_norm
         denominator = jnp.sum(q * new_norm, axis=1, keepdims=True)
         query_key = jnp.sum(q * k, axis=1, keepdims=True)
-        q_columns = q.T
+        q_lanes = dot(q.T.astype(BF16), spread)
         carried = jnp.concatenate(
             [
-                jnp.sum(q_columns[:, b : b + 1] * vmem[b, head], axis=0, keepdims=True)
+                jnp.concatenate(
+                    [
+                        jnp.sum(
+                            q_lanes[:, b * LANES : (b + 1) * LANES]
+                            * vmem[b, head, :, first : first + LANES],
+                            axis=0,
+                            keepdims=True,
+                        )
+                        for first in range(0, VD, LANES)
+                    ],
+                    axis=1,
+                )
                 for b in range(seq)
             ],
             axis=0,
@@ -294,7 +321,7 @@
     mixed = jnp.concatenate(mixed, axis=1)
     heads_all[me] = jnp.concatenate([mixed[:, :half], mixed[:, half:]], axis=0).astype(BF16)
     for target in far_first:
-        send(heads_all.at[me], heads_all.at[me], 3, recv2.at[me], {"kv": target})
+        send(heads_all.at[me], heads_all.at[me], 3, recv2.at[slot(me, target)], {"kv": target})
 
     for head in range(local_heads):
         forget, gain, scaled_key, denominator, query_key, carried = states[head]
@@ -308,28 +335,28 @@
 
     loads[6].wait()
     for source in near_first:
-        drain(heads_all.at[source], recv2.at[source])
+        drain(heads_all.at[source], recv2.at[slot(source, me)])
     gathered = [heads_all[block].astype(F32) for block in range(kv_size)]
     low = jnp.concatenate([g[:seq] for g in gathered], axis=0).astype(BF16)
     high = jnp.concatenate([g[seq:] for g in gathered], axis=0).astype(BF16)
     branch_own[...] = (dot(low, vwout[:half, :]) + dot(high, vwout[half:, :])).astype(BF16)
 
-    @pl.when(core != 0)
-    def _():
-        send(branch_own, branch_recv.at[core - 1], 4, recv3.at[core - 1], {"tp": 0})
-
-    @pl.when(core == 0)
+    @pl.when(core != lead)
+    def _():
+        send(branch_own, branch_recv.at[after_lead], 4, recv3.at[after_lead], {"tp": lead})
+
+    @pl.when(core == lead)
     def _():
         branch = branch_own[...].astype(F32)
-        for other in range(tp_size - 1):
+        for other in range(len(beside_lead)):
             drain(branch_recv.at[other], recv3.at[other])
             branch = branch + branch_recv[other].astype(F32)
         resid_all[me] = (activations + branch).astype(BF16)
-        for target in far_first:
+        for target in ends_far_first:
             send(resid_all.at[me], resid_all.at[me], 4, recv4.at[me], {"kv": target})
 
     def pass_on(source):
-        for other in range(1, tp_size):
+        for other in beside_lead:
             send(
                 resid_all.at[source],
                 resid_all.at[source],
@@ -340,15 +367,15 @@
 
     loads[7].wait()
     loads[8].wait()
-    gate_value = up_value = square_sum = 0.0
+    square_sum = 0.0
     for source in [me] + near_first:
-        @pl.when(core == 0)
+        @pl.when(core == lead)
         def _():
             if source is not me:
                 drain(resid_all.at[source], recv4.at[source])
             pass_on(source)
 
-        @pl.when(core != 0)
+        @pl.when(core != lead)
         def _():
             drain(resid_all.at[source], recv4.at[source])
 
@@ -356,68 +383,66 @@
         square_sum = square_sum + jnp.sum(block * block, axis=1, keepdims=True)
         block = (block * gain_rows[source]).astype(BF16)
         span = pl.ds(pl.multiple_of(source * cols, cols), cols)
-        gate_value = gate_value + dot_rows(block, vgate[:, span])
-        up_value = up_value + dot_rows(block, vup[:, span])
+        if source is me:
+            gate_sum_ref[...] = dot_rows(block, vgate[:, span])
+            up_sum_ref[...] = dot_rows(block, vup[:, span])
+        else:
+            gate_sum_ref[...] += dot_rows(block, vgate[:, span])
+            up_sum_ref[...] += dot_rows(block, vup[:, span])
     inverse_two = lax.rsqrt(square_sum / width + EPSILON)
-    gate_value = gate_value * inverse_two
-    up_value = up_value * inverse_two
+    gate_value = gate_sum_ref[...] * inverse_two
+    up_value = up_sum_ref[...] * inverse_two
     hidden = (gate_value * jax.nn.sigmoid(gate_value) * up_value).astype(BF16)
 
     loads[9].wait()
-    upper = me >= kv_size // 2
-    for step in range(chunks):
-        chunk = jnp.where(upper, step, chunks - 1 - step) if chunks > 1 else 0
-        span = pl.ds(pl.multiple_of(chunk * chunk_cols, chunk_cols), chunk_cols)
+    for step, chip in enumerate(far_first + [me]):
+        span = pl.ds(pl.multiple_of(chip * cols, cols), cols)
         part = dot(hidden, vdown[:, span])
 
-        @pl.when(core != last)
+        @pl.when(core != sink)
         def _():
             down_pair[step] = part.astype(BF16)
             send(
                 down_pair.at[step],
-                pair_recv.at[core, step],
+                pair_recv.at[after_sink, step],
                 6,
-                pair_sem.at[core, step],
-                {"tp": last},
+                pair_sem.at[after_sink, step],
+                {"tp": sink},
             )
 
-        @pl.when(core == last)
+        @pl.when(core == sink)
         def _():
             summed = part
-            for other in range(last):
+            for other in range(len(beside_sink)):
                 drain(pair_recv.at[other, step], pair_sem.at[other, step])
                 summed = summed + pair_recv[other, step].astype(F32)
-            for chip in range(chunk_chips):
+            for other in range(tp_size):
+                first = other * out_cols
+                down_send[chip * tp_size + other] = summed[:, first : first + out_cols].astype(BF16)
+            if chip is me:
+                for other in beside_sink:
+                    send(
+                        down_send.at[me * tp_size + other],
+                        down_recv.at[me],
+                        6,
+                        recv5.at[me],
+                        {"tp": other},
+                    )
+            else:
                 for other in range(tp_size):
-                    index = (chunk * chunk_chips + chip) * tp_size + other
-                    first = (chip * tp_size + other) * out_cols
-                    down_send[index] = summed[:, first : first + out_cols].astype(BF16)
-            base = chunk * chunk_chips
-            for place in range(chunk_chips):
-                chip = base + jnp.where(upper, place, chunk_chips - 1 - place)
-                for other in range(tp_size):
-                    block = down_send.at[chip * tp_size + other]
-
-                    @pl.when(chip != me)
-                    def _():
-                        send(
-                            block,
-                            down_recv.at[me],
-                            6,
-                            recv5.at[me],
-                            {"kv": chip, "tp": other},
-                        )
-
-                    if other != last:
-                        @pl.when(chip == me)
-                        def _():
-                            send(block, down_recv.at[me], 6, recv5.at[me], {"tp": other})
-
-    @pl.when(core == last)
-    def _():
-        down_recv[me] = down_send[me * tp_size + last]
-
-    @pl.when(core != last)
+                    send(
+                        down_send.at[chip * tp_size + other],
+                        down_recv.at[me],
+                        6,
+                        recv5.at[me],
+                        {"kv": chip, "tp": other},
+                    )
+
+    @pl.when(core == sink)
+    def _():
+        down_recv[me] = down_send[me * tp_size + sink]
+
+    @pl.when(core != sink)
     def _():
         drain(down_recv.at[me], recv5.at[me])
 
@@ -440,30 +465,31 @@
     drain(send_vo.at[:peers], send_sem.at[2])
     drain(heads_all.at[:peers], send_sem.at[3])
 
-    @pl.when(core == 0)
+    @pl.when(core == lead)
     def _():
         drain(resid_all.at[:peers], send_sem.at[4])
         for _ in range(tp_size - 1):
             drain(resid_all, send_sem.at[5])
 
-    @pl.when(core != 0)
+    @pl.when(core != lead)
     def _():
         drain(branch_own, send_sem.at[4])
 
-    @pl.when(core == last)
+    @pl.when(core == sink)
     def _():
         drain(down_send.at[: group - 1], send_sem.at[6])
 
-    @pl.when(core != last)
+    @pl.when(core != sink)
     def _():
         drain(down_pair, send_sem.at[6])
 
 
 def store_kernel(mixed, memory, normalizer, stabilizer, *rest):
     sem = rest[-1]
+    pairs = [(memory.at[i], rest[1].at[i]) for i in range(memory.shape[0])]
+    pairs += [(mixed, rest[0]), (normalizer, rest[2]), (stabilizer, rest[3])]
     copies = [
-        pltpu.make_async_copy(src, dst, sem.at[i])
-        for i, (src, dst) in enumerate(zip((mixed, memory, normalizer, stabilizer), rest))
+        pltpu.make_async_copy(src, dst, sem.at[i]) for i, (src, dst) in enumerate(pairs)
     ]
     for copy in copies:
         copy.start()
@@ -500,7 +526,7 @@
     vmem = pl.BlockSpec(memory_space=pltpu.VMEM)
     hbm = pl.BlockSpec(memory_space=pl.ANY)
     width = cols * kv_size
-    chunks = 2 if kv_size % 2 == 0 else 1
+    chunks = kv_size
 
     def like(array):
         return pltpu.VMEM(array.shape, array.dtype)
@@ -546,6 +572,8 @@
             pltpu.VMEM((max(tp_size - 1, 1), rows, cols), BF16),
             pltpu.VMEM((kv_size, rows, cols), BF16),
             pltpu.VMEM((kv_size, 1, cols), F32),
+            pltpu.VMEM((rows, w_gate.shape[0]), F32),
+            pltpu.VMEM((rows, w_up.shape[0]), F32),
             pltpu.VMEM((chunks, rows, width // chunks), BF16),
             pltpu.VMEM((max(tp_size - 1, 1), chunks, rows, width // chunks), BF16),
             pltpu.VMEM((group, rows, out_cols), BF16),
@@ -553,8 +581,8 @@
             pltpu.SemaphoreType.DMA((10,)),
             pltpu.SemaphoreType.DMA((7,)),
             pltpu.SemaphoreType.DMA((7,)),
-            pltpu.SemaphoreType.DMA((3, kv_size)),
-            pltpu.SemaphoreType.DMA((kv_size,)),
+            pltpu.SemaphoreType.DMA((3, kv_size - 1)),
+            pltpu.SemaphoreType.DMA((kv_size - 1,)),
             pltpu.SemaphoreType.DMA((max(tp_size - 1, 1),)),
             pltpu.SemaphoreType.DMA((kv_size,)),
             pltpu.SemaphoreType.DMA((max(tp_size - 1, 1), chunks)),
@@ -587,7 +615,7 @@
         out_shape=tuple(jax.ShapeDtypeStruct(*result) for result in results),
         in_specs=[vmem] * len(results),
         out_specs=(hbm,) * len(results),
-        scratch_shapes=[pltpu.SemaphoreType.DMA((len(results),))],
+        scratch_shapes=[pltpu.SemaphoreType.DMA((seq + len(results) - 1,))],
         compiler_params=pltpu.CompilerParams(vmem_limit_bytes=2**20),
     )(*held)
     return mixed_out, new_memory, new_normalizer, new_stabilizer.T

time: 28.6 us -> 26.8 us (0.937)
  Pallas kernels: 27.8 us -> 26 us
    pallas_call x1, Pallas kernels: 25.7 us -> 23.9 us  [body(): pl.pallas_call(functools.partial(layer_kernel, kv_size, tp_size), out_sha...]
where the time goes in v2:
time: 26.8 us; the launch traced here: 26.7 us
  Pallas kernels  26 us (97%)
  between operations  0.65 us (2%)
    pallas_call x1, Pallas kernels, body(): pl.pallas_call(functools.partial(layer_kernel, kv_size, tp_size), out_sha...  23.9 us
    pallas_call x1, Pallas kernels, body(): pl.pallas_call(store_kernel, out_shape=tuple((jax.ShapeDtypeStruct(*resul...  2.11 us

profile of v2, /device:TPU:0, one launch (start us, length us, event | category | flops | bytes accessed | tf_op | source)
XLA Modules:
  0.0 26.7 jit_solution(10648454947485687646)
XLA Ops:
  0.6 23.9 %shard_map.192 = (bf16[32,256]{1,0:T(8,128)(2,1)S(1)}, f32[8,4,128,256]{3,2,1,0:T(8,128)S(1)}, f32[8,4,128]{2,1,0:T(4,128)S(1)}, f32[4,8]{1,0:T(4,128)S(1)}) custom-call(bf16[32,512]{1,0:T(8,128)(2,1)} %tokens_in.1, f32[1,512]{1,0:T(1,128)} %bitcast.12, bf16[512,512]{1,0:T(8,128)(2,1)} %w_query.1, bf16[512,512]{1,0:T(8,128)(2,1)} %w_key.1, ...), custom_call_target="tpu_custom_call" | custom-call | tf_op jit(solution)/shard_map/pallas_call | solution.py:542
  24.6 2.1 %shard_map.193 = (bf16[32,256]{1,0:T(8,128)(2,1)}, f32[8,4,128,256]{3,2,1,0:T(8,128)}, f32[8,4,128]{2,1,0:T(4,128)}, f32[4,8]{1,0:T(4,128)}) custom-call(bf16[32,256]{1,0:T(8,128)(2,1)S(1)} %get-tuple-element.12.mixed, f32[8,4,128,256]{3,2,1,0:T(8,128)S(1)} %get-tuple-element.13.memory, f32[8,4,128]{2,1,0:T(4,128)S(1)} %get-tuple-element.14.normalizer, ...), custom_call_target="tpu_custom_call" | custom-call | tf_op jit(solution)/shard_map/pallas_call | solution.py:613

commit v3 on v2

--- a/solution.py
+++ b/solution.py
@@ -92,6 +92,7 @@
     small_sem,
     send_sem,
     recv1,
+    recv_gates_sem,
     recv2,
     recv3,
     recv4,
@@ -105,6 +106,7 @@
     width = cols * kv_size
     local_heads = forget_bias.shape[1]
     total_heads = local_heads * tp_size
+    peers = kv_size - 1
     half = local_heads * VD // 2
     group = kv_size * tp_size
     out_cols = width // group
@@ -115,16 +117,13 @@
     after_lead = lax.rem(core + tp_size - lead - 1 + tp_size, tp_size)
     after_sink = lax.rem(core + tp_size - sink - 1 + tp_size, tp_size)
 
+    far_first = [nearest(k, me, kv_size) for k in range(kv_size - 1, 0, -1)]
+    near_first = far_first[::-1]
     barrier = pltpu.get_barrier_semaphore()
-    rank = me * tp_size + core
-    for step in range(1, group):
-        other = lax.rem(rank + step, group)
-        pl.semaphore_signal(
-            barrier,
-            inc=1,
-            device_id={"kv": other // tp_size, "tp": lax.rem(other, tp_size)},
-            device_id_type=MESH,
-        )
+    entered = [{"kv": chip, "tp": other} for chip in far_first for other in range(tp_size)]
+    entered += [{"tp": lax.rem(core + step, tp_size)} for step in range(1, tp_size)]
+    for device in entered:
+        pl.semaphore_signal(barrier, inc=1, device_id=device, device_id_type=MESH)
 
     loads = [
         pltpu.make_async_copy(src, dst, load_sem.at[i])
@@ -157,8 +156,10 @@
             )
         )
     ]
-    for load in small[:2] + loads[:5] + small[2:]:
+    for load in small[:2] + loads[:3]:
         load.start()
+    for load in loads[3:5] + small[2:]:
+        load.start(priority=1)
 
     def send(src, dst, index, recv_sem, device):
         pltpu.make_async_remote_copy(
@@ -176,10 +177,7 @@
     def drain(ref, sem):
         pltpu.make_async_copy(ref, ref, sem).wait()
 
-    far_first = [nearest(k, me, kv_size) for k in range(kv_size - 1, 0, -1)]
-    near_first = far_first[::-1]
-    outer = jnp.minimum(me, kv_size - 1 - me) < kv_size // 4
-    ends_far_first = [jnp.where(outer, a, b) for a, b in zip(far_first, near_first)]
+    rising = [jnp.where(chip < me, chip, chip + 1) for chip in range(kv_size - 1)]
 
     small[0].wait()
     small[1].wait()
@@ -194,7 +192,7 @@
 
     def scatter(buffer, landing, kind):
         for target in far_first:
-            send(buffer.at[target], landing.at[me], kind, recv1.at[kind, slot(me, target)], {"kv": target})
+            send(buffer.at[target], landing.at[me] if kind else landing.at[slot(me, target)], kind, recv1.at[kind - 1, slot(me, target)] if kind else recv_gates_sem, {"kv": target})
 
     loads[0].wait()
     gate_part = dot_rows(scaled, vgates[...])
@@ -234,11 +232,14 @@
     def total(buffer, landing, kind):
         result = buffer[me].astype(F32)
         for source in near_first:
-            drain(landing.at[source], recv1.at[kind, slot(source, me)])
+            drain(landing.at[source], recv1.at[kind - 1, slot(source, me)])
             result = result + landing[source].astype(F32)
         return result
 
-    gate_sum = total(send_gs, recv_gs, 0)
+    drain(recv_gs, recv_gates_sem)
+    gate_sum = send_gs[me]
+    for peer in range(peers):
+        gate_sum = gate_sum + recv_gs[peer]
 
     inverse = lax.rsqrt(gate_sum[:, 2 * total_heads : 2 * total_heads + 1] / width + EPSILON)
     gate_pre = gate_sum[:, : 2 * total_heads] * inverse
@@ -321,7 +322,7 @@
     mixed = jnp.concatenate(mixed, axis=1)
     heads_all[me] = jnp.concatenate([mixed[:, :half], mixed[:, half:]], axis=0).astype(BF16)
     for target in far_first:
-        send(heads_all.at[me], heads_all.at[me], 3, recv2.at[slot(me, target)], {"kv": target})
+        send(heads_all.at[me], heads_all.at[me], 3, recv2, {"kv": target})
 
     for head in range(local_heads):
         forget, gain, scaled_key, denominator, query_key, carried = states[head]
@@ -334,8 +335,7 @@
             )
 
     loads[6].wait()
-    for source in near_first:
-        drain(heads_all.at[source], recv2.at[slot(source, me)])
+    drain(heads_all.at[:peers], recv2)
     gathered = [heads_all[block].astype(F32) for block in range(kv_size)]
     low = jnp.concatenate([g[:seq] for g in gathered], axis=0).astype(BF16)
     high = jnp.concatenate([g[seq:] for g in gathered], axis=0).astype(BF16)
@@ -352,7 +352,7 @@
             drain(branch_recv.at[other], recv3.at[other])
             branch = branch + branch_recv[other].astype(F32)
         resid_all[me] = (activations + branch).astype(BF16)
-        for target in ends_far_first:
+        for target in rising[::-1]:
             send(resid_all.at[me], resid_all.at[me], 4, recv4.at[me], {"kv": target})
 
     def pass_on(source):
@@ -395,7 +395,7 @@
     hidden = (gate_value * jax.nn.sigmoid(gate_value) * up_value).astype(BF16)
 
     loads[9].wait()
-    for step, chip in enumerate(far_first + [me]):
+    for step, chip in enumerate(rising + [me]):
         span = pl.ds(pl.multiple_of(chip * cols, cols), cols)
         part = dot(hidden, vdown[:, span])
 
@@ -459,7 +459,6 @@
         drain(down_recv.at[source], recv5.at[source])
         summed = summed + down_recv[source].astype(F32)
     out_mixed[...] = summed.astype(BF16)
-    peers = kv_size - 1
     drain(send_gs.at[:peers], send_sem.at[0])
     drain(send_qk.at[:peers], send_sem.at[1])
     drain(send_vo.at[:peers], send_sem.at[2])
@@ -566,7 +565,7 @@
             pltpu.VMEM((kv_size, seq, 128), F32),
             pltpu.VMEM((kv_size, 2 * seq, local_heads * QK), BF16),
             pltpu.VMEM((kv_size, 2 * seq, local_heads * VD), BF16),
-            pltpu.VMEM((kv_size, seq, 128), F32),
+            pltpu.VMEM((kv_size - 1, seq, 128), F32),
             pltpu.VMEM((kv_size, 2 * seq, half), BF16),
             pltpu.VMEM((rows, cols), BF16),
             pltpu.VMEM((max(tp_size - 1, 1), rows, cols), BF16),
@@ -581,8 +580,9 @@
             pltpu.SemaphoreType.DMA((10,)),
             pltpu.SemaphoreType.DMA((7,)),
             pltpu.SemaphoreType.DMA((7,)),
-            pltpu.SemaphoreType.DMA((3, kv_size - 1)),
-            pltpu.SemaphoreType.DMA((kv_size - 1,)),
+            pltpu.SemaphoreType.DMA((2, kv_size - 1)),
+            pltpu.SemaphoreType.DMA,
+            pltpu.SemaphoreType.DMA,
             pltpu.SemaphoreType.DMA((max(tp_size - 1, 1),)),
             pltpu.SemaphoreType.DMA((kv_size,)),
             pltpu.SemaphoreType.DMA((max(tp_size - 1, 1), chunks)),

time: 26.8 us -> 26.5 us (0.989)
  Pallas kernels: 26 us -> 25.7 us
    pallas_call x1, Pallas kernels: 23.9 us -> 23.6 us  [body(): pl.pallas_call(functools.partial(layer_kernel, kv_size, tp_size), out_sha...]
where the time goes in v3:
time: 26.5 us; the launch traced here: 26.4 us
  Pallas kernels  25.7 us (97%)
  between operations  0.65 us (2%)
    pallas_call x1, Pallas kernels, body(): pl.pallas_call(functools.partial(layer_kernel, kv_size, tp_size), out_sha...  23.6 us
    pallas_call x1, Pallas kernels, body(): pl.pallas_call(store_kernel, out_shape=tuple((jax.ShapeDtypeStruct(*resul...  2.11 us

profile of v3, /device:TPU:0, one launch (start us, length us, event | category | flops | bytes accessed | tf_op | source)
XLA Modules:
  0.0 26.4 jit_solution(11726141382189487381)
XLA Ops:
  0.6 23.6 %shard_map.192 = (bf16[32,256]{1,0:T(8,128)(2,1)S(1)}, f32[8,4,128,256]{3,2,1,0:T(8,128)S(1)}, f32[8,4,128]{2,1,0:T(4,128)S(1)}, f32[4,8]{1,0:T(4,128)S(1)}) custom-call(bf16[32,512]{1,0:T(8,128)(2,1)} %tokens_in.1, f32[1,512]{1,0:T(1,128)} %bitcast.12, bf16[512,512]{1,0:T(8,128)(2,1)} %w_query.1, bf16[512,512]{1,0:T(8,128)(2,1)} %w_key.1, ...), custom_call_target="tpu_custom_call" | custom-call | tf_op jit(solution)/shard_map/pallas_call | solution.py:541
  24.3 2.1 %shard_map.193 = (bf16[32,256]{1,0:T(8,128)(2,1)}, f32[8,4,128,256]{3,2,1,0:T(8,128)}, f32[8,4,128]{2,1,0:T(4,128)}, f32[4,8]{1,0:T(4,128)}) custom-call(bf16[32,256]{1,0:T(8,128)(2,1)S(1)} %get-tuple-element.12.mixed, f32[8,4,128,256]{3,2,1,0:T(8,128)S(1)} %get-tuple-element.13.memory, f32[8,4,128]{2,1,0:T(4,128)S(1)} %get-tuple-element.14.normalizer, ...), custom_call_target="tpu_custom_call" | custom-call | tf_op jit(solution)/shard_map/pallas_call | solution.py:613

commit v4 on v3

--- a/solution.py
+++ b/solution.py
@@ -79,6 +79,7 @@
     recv_gs,
     heads_all,
     branch_own,
+    branch_sum,
     branch_recv,
     resid_all,
     gain_rows,
@@ -319,10 +320,18 @@
             * head_gain[head : head + 1, :]
         )
         mixed.append(normed * jax.nn.sigmoid(outgate[:, span]))
-    mixed = jnp.concatenate(mixed, axis=1)
-    heads_all[me] = jnp.concatenate([mixed[:, :half], mixed[:, half:]], axis=0).astype(BF16)
-    for target in far_first:
-        send(heads_all.at[me], heads_all.at[me], 3, recv2, {"kv": target})
+        if (head + 1) * VD % half == 0:
+            part = (head + 1) * VD // half - 1
+            heads_all[part, me] = jnp.concatenate(mixed, axis=1).astype(BF16)
+            mixed = []
+            for target in far_first:
+                send(
+                    heads_all.at[part, me],
+                    heads_all.at[part, me],
+                    3,
+                    recv2.at[part],
+                    {"kv": target},
+                )
 
     for head in range(local_heads):
         forget, gain, scaled_key, denominator, query_key, carried = states[head]
@@ -335,11 +344,14 @@
             )
 
     loads[6].wait()
-    drain(heads_all.at[:peers], recv2)
-    gathered = [heads_all[block].astype(F32) for block in range(kv_size)]
-    low = jnp.concatenate([g[:seq] for g in gathered], axis=0).astype(BF16)
-    high = jnp.concatenate([g[seq:] for g in gathered], axis=0).astype(BF16)
-    branch_own[...] = (dot(low, vwout[:half, :]) + dot(high, vwout[half:, :])).astype(BF16)
+    for part in range(2):
+        drain(heads_all.at[part, :peers], recv2.at[part])
+        gathered = [heads_all[part, block].astype(F32) for block in range(kv_size)]
+        gathered = jnp.concatenate(gathered, axis=0).astype(BF16)
+        if part == 0:
+            branch_sum[...] = dot(gathered, vwout[:half, :])
+        else:
+            branch_own[...] = (branch_sum[...] + dot(gathered, vwout[half:, :])).astype(BF16)
 
     @pl.when(core != lead)
     def _():
@@ -462,7 +474,7 @@
     drain(send_gs.at[:peers], send_sem.at[0])
     drain(send_qk.at[:peers], send_sem.at[1])
     drain(send_vo.at[:peers], send_sem.at[2])
-    drain(heads_all.at[:peers], send_sem.at[3])
+    drain(heads_all.at[:, :peers], send_sem.at[3])
 
     @pl.when(core == lead)
     def _():
@@ -566,8 +578,9 @@
             pltpu.VMEM((kv_size, 2 * seq, local_heads * QK), BF16),
             pltpu.VMEM((kv_size, 2 * seq, local_heads * VD), BF16),
             pltpu.VMEM((kv_size - 1, seq, 128), F32),
-            pltpu.VMEM((kv_size, 2 * seq, half), BF16),
+            pltpu.VMEM((2, kv_size, seq, half), BF16),
             pltpu.VMEM((rows, cols), BF16),
+            pltpu.VMEM((rows, cols), F32),
             pltpu.VMEM((max(tp_size - 1, 1), rows, cols), BF16),
             pltpu.VMEM((kv_size, rows, cols), BF16),
             pltpu.VMEM((kv_size, 1, cols), F32),
@@ -582,7 +595,7 @@
             pltpu.SemaphoreType.DMA((7,)),
             pltpu.SemaphoreType.DMA((2, kv_size - 1)),
             pltpu.SemaphoreType.DMA,
-            pltpu.SemaphoreType.DMA,
+            pltpu.SemaphoreType.DMA((2,)),
             pltpu.SemaphoreType.DMA((max(tp_size - 1, 1),)),
             pltpu.SemaphoreType.DMA((kv_size,)),
             pltpu.SemaphoreType.DMA((max(tp_size - 1, 1), chunks)),

time: 26.5 us -> 26.6 us (level)
  no operation moved by 1% of the time
where the time goes in v4:
time: 26.6 us; the launch traced here: 26.4 us
  Pallas kernels  25.8 us (97%)
  between operations  0.65 us (2%)
    pallas_call x1, Pallas kernels, body(): pl.pallas_call(functools.partial(layer_kernel, kv_size, tp_size), out_sha...  23.7 us
    pallas_call x1, Pallas kernels, body(): pl.pallas_call(store_kernel, out_shape=tuple((jax.ShapeDtypeStruct(*resul...  2.11 us

profile of v4, /device:TPU:0, one launch (start us, length us, event | category | flops | bytes accessed | tf_op | source)
XLA Modules:
  0.0 26.4 jit_solution(9753604623775941319)
XLA Ops:
  0.6 23.7 %shard_map.192 = (bf16[32,256]{1,0:T(8,128)(2,1)S(1)}, f32[8,4,128,256]{3,2,1,0:T(8,128)S(1)}, f32[8,4,128]{2,1,0:T(4,128)S(1)}, f32[4,8]{1,0:T(4,128)S(1)}) custom-call(bf16[32,512]{1,0:T(8,128)(2,1)} %tokens_in.1, f32[1,512]{1,0:T(1,128)} %bitcast.12, bf16[512,512]{1,0:T(8,128)(2,1)} %w_query.1, bf16[512,512]{1,0:T(8,128)(2,1)} %w_key.1, ...), custom_call_target="tpu_custom_call" | custom-call | tf_op jit(solution)/shard_map/pallas_call | solution.py:553
  24.3 2.1 %shard_map.193 = (bf16[32,256]{1,0:T(8,128)(2,1)}, f32[8,4,128,256]{3,2,1,0:T(8,128)}, f32[8,4,128]{2,1,0:T(4,128)}, f32[4,8]{1,0:T(4,128)}) custom-call(bf16[32,256]{1,0:T(8,128)(2,1)S(1)} %get-tuple-element.12.mixed, f32[8,4,128,256]{3,2,1,0:T(8,128)S(1)} %get-tuple-element.13.memory, f32[8,4,128]{2,1,0:T(4,128)S(1)} %get-tuple-element.14.normalizer, ...), custom_call_target="tpu_custom_call" | custom-call | tf_op jit(solution)/shard_map/pallas_call | solution.py:626
